TPU v7x, 32 devices: a whole 2x2x4 slice. The times are simulated.
32 devices in a mesh: rep: 2 (over x), fs: 8 (over z, y), tp: 2 (over core).
Axes of the slice: x: 2, y: 2, z: 4, core: 2. Of those that a mesh axis runs over, the one named last changes fastest.
Arguments:
- tokens: bfloat16 [16384, 2048], P(('rep', 'fs', 'tp')), may hold values from -6 to 6
- pre_gain: bfloat16 [2048], replicated, may hold values from 0.099609375 to 1.8984375
- gate_weight: bfloat16 [2048, 2816], P('fs', 'tp'), may hold values from -0.125 to 0.125
- value_weight: bfloat16 [2048, 2816], P('fs', 'tp'), may hold values from -0.125 to 0.125
- down_weight: bfloat16 [2816, 2048], P('tp', 'fs'), may hold values from -0.109375 to 0.109375
- post_gain: bfloat16 [2048], replicated, may hold values from 0.099609375 to 1.8984375
Outputs:
- updated: bfloat16 [16384, 2048], P(('rep', 'fs', 'tp'))
All inputs are finite; a program needn't handle non-finite values.
Results may differ from a plain program's by a relative error of at most 0.0055.
Values may be sent and summed in bfloat16 or wider, within the bound.
A program may use at most 128 MiB of HBM per device.

v0:
```python
import jax
import jax.numpy as jnp
from jax import lax
from jax.sharding import PartitionSpec as P

eps_norm = 1e-06


def rms_rows(values_in, gain):
    floats = values_in.astype(jnp.float32)
    scaled = floats * lax.rsqrt(jnp.mean(floats * floats, -1, keepdims=True) + eps_norm)
    return scaled * gain.astype(jnp.float32)


def shards(tokens, pre_gain, gate_weight, value_weight, down_weight, post_gain):
    normed = rms_rows(tokens, pre_gain).astype(jnp.bfloat16)
    group_rows = lax.all_gather(normed, "tp", axis=0, tiled=True)
    gate_add = jnp.dot(
        group_rows,
        lax.all_gather(gate_weight, "fs", axis=0, tiled=True),
        preferred_element_type=jnp.float32,
    )
    value_add = jnp.dot(
        group_rows,
        lax.all_gather(value_weight, "fs", axis=0, tiled=True),
        preferred_element_type=jnp.float32,
    )
    down_full = lax.all_gather(down_weight, "fs", axis=1, tiled=True)
    hidden = (jax.nn.silu(gate_add) * value_add).astype(jnp.bfloat16)
    branch = lax.psum_scatter(
        jnp.dot(hidden, down_full, preferred_element_type=jnp.float32).astype(jnp.bfloat16),
        "tp",
        scatter_dimension=0,
        tiled=True,
    )
    updated = tokens.astype(jnp.float32) + 0.5 * rms_rows(branch, post_gain)
    return updated.astype(jnp.bfloat16)


def solution(mesh):
    placed = (P(("rep", "fs", "tp"), None), P(), P("fs", "tp"), P("fs", "tp"), P("tp", "fs"), P())
    return jax.shard_map(
        shards, mesh=mesh, in_specs=placed, out_specs=P(("rep", "fs", "tp"), None), check_vma=False
    )
```

profile of v0, /device:TPU:1, one launch (start us, length us, event | category | flops | bytes accessed | tf_op | source)
XLA Modules:
  0.0 354.5 jit_solution(6373877457626847716)
XLA Ops:
  6.5 0.0 all-gather.5.cloned.1.call-start
  6.5 0.7 convert_element_type.26
  7.2 2.1 fusion.3
  9.3 3.5 fusion.5
  12.8 0.0 all-gather.5.cloned.1.call-update
  12.8 0.0 all-gather.7.cloned.1.call-start
  12.8 0.7 all-gather.7.cloned.1.call-update
  13.6 0.0 all-gather.11.cloned.1.call-start
  13.6 0.7 all-gather.11.cloned.1.call-update
  14.3 0.0 all-gather.9.cloned.1.call-start
  14.3 0.5 all-gather.9.cloned.1.call-update
  14.9 0.0 reduce-scatter.2.cloned.1.call-start
  14.9 14.2 %all-gather.5.cloned.1.call-done = bf16[1024,2048]{1,0:T(8,128)(2,1)} async-done(((bf16[512,2048]{1,0:T(8,128)(2,1)}), bf16[1024,2048]{1,0:T(8,128)(2,1)}) %all-gather.5.cloned.1.call-update) | async-done | bytes 4194320 | tf_op jit(solution)/shard_map/all_gather | solution.py:17
  29.1 93.8 %all-gather.7.cloned.1.call-done = bf16[2048,1408]{1,0:T(8,128)(2,1)} async-done(((bf16[256,1408]{1,0:T(8,128)(2,1)}), bf16[2048,1408]{1,0:T(8,128)(2,1)}) %all-gather.7.cloned.1.call-update) | async-done | bytes 5767184 | tf_op jit(solution)/shard_map/all_gather | solution.py:20
  122.9 11.7 %fusion.7 = f32[1024,1408]{1,0:T(8,128)} fusion(bf16[1024,2048]{1,0:T(8,128)(2,1)} %all-gather.5.cloned.1.call-done, bf16[2048,1408]{1,0:T(8,128)(2,1)} %all-gather.7.cloned.1.call-done), kind=kOutput, calls=%fused_computation.16 | convolution fusion | flops 5905580032 | bytes 15728640 | tf_op jit(solution)/shard_map/dot_general | solution.py:18
  134.5 82.5 %all-gather.11.cloned.1.call-done = bf16[1408,2048]{1,0:T(8,128)(2,1)} async-done(((bf16[1408,256]{1,0:T(8,128)(2,1)}), bf16[1408,2048]{1,0:T(8,128)(2,1)}) %all-gather.11.cloned.1.call-update) | async-done | bytes 5767184 | tf_op jit(solution)/shard_map/all_gather | solution.py:28
  217.0 91.8 %all-gather.9.cloned.1.call-done = bf16[2048,1408]{1,0:T(8,128)(2,1)} async-done(((bf16[256,1408]{1,0:T(8,128)(2,1)}), bf16[2048,1408]{1,0:T(8,128)(2,1)}) %all-gather.9.cloned.1.call-update) | async-done | bytes 5767184 | tf_op jit(solution)/shard_map/all_gather | solution.py:25
  308.8 20.6 %convolution_convert_fusion = bf16[1024,2048]{1,0:T(8,128)(2,1)} fusion(bf16[1408,2048]{1,0:T(8,128)(2,1)} %all-gather.11.cloned.1.call-done, f32[1024,1408]{1,0:T(8,128)} %fusion.7, bf16[1024,2048]{1,0:T(8,128)(2,1)} %all-gather.5.cloned.1.call-done, bf16[2048,1408]{1,0:T(8,128)(2,1)} %all-gather.9.cloned.1.call-done), kind=kOutput, calls=%fused_computation.13 | convolution fusion | flops 11821907968 | bytes 25690112 | tf_op jit(solution)/shard_map/dot_general | solution.py:31
  329.4 0.0 copy-start.1
  329.4 0.0 copy-start
  329.4 0.0 reduce-scatter.2.cloned.1.call-update
  329.4 0.7 copy-done.1
  330.1 11.7 %reduce-scatter.2.cloned.1.call-done = bf16[512,2048]{1,0:T(8,128)(2,1)} async-done(((bf16[1024,2048]{1,0:T(8,128)(2,1)}), bf16[512,2048]{1,0:T(8,128)(2,1)}) %reduce-scatter.2.cloned.1.call-update) | async-done | bytes 2097168 | tf_op jit(solution)/shard_map/reduce_scatter | solution.py:30
  341.8 2.1 fusion
  343.9 0.0 copy-done
  343.9 4.0 %fusion.6 = bf16[512,2048]{1,0:T(8,128)(2,1)} fusion(bf16[512,2048]{1,0:T(8,128)(2,1)} %reduce-scatter.2.cloned.1.call-done, bf16[512,2048]{1,0:T(8,128)(2,1)S(1)} %copy-done, f32[2048]{0:T(1024)S(1)} %convert_element_type.31, f32[512]{0:T(512)S(1)} %add_rsqrt_fusion), kind=kLoop, calls=%fused_computation.12 | loop fusion | flops 7340032 | bytes 6301696 | tf_op jit(solution)/shard_map/convert_element_type | solution.py:37
  (3 shorter events, 0.0 us)
Async XLA Ops:
  6.5 22.5 %all-gather.5.cloned.1.call-start = ((), (), s32[]{:S(2)}) async-start(), calls=%async_computation.1 | async-start | bytes 6291456 | tf_op jit(solution)/shard_map/all_gather | solution.py:17
  12.8 110.1 %all-gather.7.cloned.1.call-start = ((), (), s32[]{:S(2)}) async-start(), calls=%async_computation.2 | async-start | bytes 6488064 | tf_op jit(solution)/shard_map/all_gather | solution.py:20
  13.6 203.5 %all-gather.11.cloned.1.call-start = ((), (), s32[]{:S(2)}) async-start(), calls=%async_computation.4 | async-start | bytes 6488064 | tf_op jit(solution)/shard_map/all_gather | solution.py:28
  14.3 294.5 %all-gather.9.cloned.1.call-start = ((), (), s32[]{:S(2)}) async-start(), calls=%async_computation.3 | async-start | bytes 6488064 | tf_op jit(solution)/shard_map/all_gather | solution.py:25
  14.9 327.0 %reduce-scatter.2.cloned.1.call-start = ((), (), s32[]{:S(2)}) async-start(), calls=%async_computation.5 | async-start | bytes 6291456 | tf_op jit(solution)/shard_map/reduce_scatter | solution.py:30
  329.4 0.7 copy-start.1
  329.4 14.5 %copy-start = (bf16[512,2048]{1,0:T(8,128)(2,1)S(1)}, bf16[512,2048]{1,0:T(8,128)(2,1)}, u32[]{:S(2)}) copy-start(bf16[512,2048]{1,0:T(8,128)(2,1)} %param.6) | copy-start | bytes 6291460
Sparse Core Ops, SparseCore 0:
  12.9 16.1 all-gather.4
  31.2 91.5 all-gather.6
  124.9 92.0 all-gather.10
  219.1 89.7 all-gather.8
  329.6 12.2 reduce-scatter.1
where the time goes:
time: 355 us; the launch traced here: 354 us
  waiting for transfers between devices  296 us (83%)
  matrix products  32.2 us (9%)
  between operations  13.2 us (4%)
  other arithmetic  12.4 us (3%)
    all_gather x1, waiting for transfers between devices, shards(): lax.all_gather(gate_weight, 'fs', axis=0, tiled=True)  93.8 us
    all_gather x1, waiting for transfers between devices, shards(): lax.all_gather(value_weight, 'fs', axis=0, tiled=True)  91.8 us
    all_gather x1, waiting for transfers between devices, shards(): down_full = lax.all_gather(down_weight, 'fs', axis=1, tiled=True)  82.5 us
    dot_general x1, matrix products, shards(): jnp.dot(hidden, down_full, preferred_element_type=jnp.float32)  20.6 us
    all_gather x1, waiting for transfers between devices, shards(): group_rows = lax.all_gather(normed, 'tp', axis=0, tiled=True)  14.2 us
    reduce_scatter x1, waiting for transfers between devices, shards(): lax.psum_scatter(jnp.dot(hidden, down_full, preferred_element_type=jnp.fl...  11.7 us
    dot_general x1, matrix products, shards(): jnp.dot(group_rows, lax.all_gather(gate_weight, 'fs', axis=0, tiled=True)...  11.7 us
  transfers between devices with their start and end apart: 5, of which 5 were waited for; matrix products, arithmetic and copies ran while one was open for 3% of the time, Pallas kernels for 0%

commit v1 on v0

v1 whole, which is shorter than its diff:
```python
import functools

import jax
import jax.numpy as jnp
from jax import lax
from jax.experimental import pallas as pl
from jax.experimental.pallas import tpu as pltpu
from jax.sharding import PartitionSpec as P

eps_norm = 1e-06
MESH = pl.DeviceIdType.MESH
f32 = jnp.float32
bf16 = jnp.bfloat16


def third(rows):
    return max(rows // 3 // 16, 1) * 16


def half_of(rows):
    return (rows // 2 + 15) // 16 * 16


def when(condition, action):
    if isinstance(condition, bool):
        if condition:
            action()
    else:
        pl.when(condition)(action)


def kernel(
    n, tok_ref, pre_ref, post_ref, g_ref, v_ref, d_ref, out_ref,
    gbuf, vbuf, dbuf, nbuf, peer, gacc, vacc, hid, precv,
    send_sem, recv_sem, tok_sem, part_send, part_recv, own_sem,
):
    T, D = tok_ref.shape
    R = gbuf.shape[1]
    F = dbuf.shape[1]
    half = n // 2
    rep = lax.axis_index("rep")
    me = lax.axis_index("fs")
    core = lax.axis_index("tp")
    odd = me % 2
    pos = (1 - odd) * (me // 2) + odd * (n - 1 - me // 2)

    def fs_at(at):
        late = at // half
        return (1 - late) * 2 * at + late * (2 * (n - 1 - at) + 1)

    right = fs_at((pos + 1) % n)
    left = fs_at((pos + n - 1) % n)
    other_rep = 1 - rep
    other_core = 1 - core

    def origin(k):
        return fs_at((pos + 2 * n - 1 - k) % n)

    a, b = third(R), third(F)
    b0, c0 = half_of(b), half_of(F - 2 * b)
    chunks = (
        (gbuf, a, 0, a, 2 * a, R - 2 * a),
        (vbuf, a, 0, a, 2 * a, R - 2 * a),
        (dbuf, b, 0, b0, 2 * b, c0),
        (dbuf, b, b0, b - b0, 2 * b + c0, F - 2 * b - c0),
    )

    def part(c, k, which):
        buf, size, start, length = chunks[c][:4]
        return buf.at[k, pl.ds(pl.multiple_of(which * size + start, 16), length)]

    def common(c, k):
        return chunks[c][0].at[k, pl.ds(chunks[c][4], chunks[c][5])]

    def remote(src, dst, way, c, s, to):
        return pltpu.make_async_remote_copy(
            src_ref=src, dst_ref=dst, send_sem=send_sem.at[way, c, s], recv_sem=recv_sem.at[way, c, s],
            device_id=to, device_id_type=MESH,
        )

    def cw(s, c):
        return remote(part(c, (s + n - 1) % n, rep), part(c, s, rep), 0, c, s, {"fs": right})

    def ccw(s, c):
        return remote(common(c, n - 1 - s), common(c, n - 2 - s), 1, c, s, {"fs": left})

    def cross(s, c):
        return remote(part(c, s, rep), part(c, s, rep), 2, c, s, {"rep": other_rep})

    def cross_in(s, c):
        return remote(part(c, s, other_rep), part(c, s, other_rep), 2, c, s, {"rep": other_rep})

    def pump(s, c):
        more = s < n - 2
        cw(s, c).wait_recv()
        when(more, lambda: cw(s + 1, c).start())
        cross(s, c).start()
        ccw(s, c).wait_recv()
        when(more, lambda: ccw(s + 1, c).start())

    def tok_copy():
        return pltpu.make_async_remote_copy(
            src_ref=tok_ref, dst_ref=peer, send_sem=tok_sem.at[0], recv_sem=tok_sem.at[1],
            device_id={"tp": other_core}, device_id_type=MESH,
        )

    def part_copy(j):
        return pltpu.make_async_remote_copy(
            src_ref=nbuf.at[j, pl.ds(T, T)], dst_ref=precv.at[j], send_sem=part_send.at[j],
            recv_sem=part_recv.at[j], device_id={"tp": other_core}, device_id_type=MESH,
        )

    own = [
        pltpu.make_async_copy(src, buf.at[n - 1], own_sem.at[i])
        for i, (src, buf) in enumerate(((g_ref, gbuf), (v_ref, vbuf), (d_ref, dbuf)))
    ]
    for copy in own:
        copy.start()

    barrier = pltpu.get_barrier_semaphore()
    for to in ({"fs": right}, {"fs": left}, {"rep": other_rep}, {"tp": other_core}):
        pl.semaphore_signal(barrier, inc=1, device_id=to, device_id_type=MESH)
    pl.semaphore_wait(barrier, 4)

    for c in range(4):
        if c < 3:
            own[c].wait()
        cw(0, c).start()
        ccw(0, c).start()
    tok_copy().start()

    rows_n = 64

    def norm_rows(src, base):
        @pl.loop(0, T // rows_n)
        def _(i):
            at = pl.ds(pl.multiple_of(i * rows_n, rows_n), rows_n)
            x = src[at, :].astype(f32)
            x = x * lax.rsqrt(jnp.mean(x * x, -1, keepdims=True) + eps_norm) * pre_ref[...].astype(f32)
            x = x.astype(bf16)
            to = pl.ds(pl.multiple_of(base + i * rows_n, rows_n), rows_n)
            for j in range(n):
                nbuf[j, to, :] = x[:, j * R:(j + 1) * R]

    norm_rows(tok_ref, 0)

    @pl.loop(0, 2 * T // rows_n)
    def _(i):
        at = pl.ds(pl.multiple_of(i * rows_n, rows_n), rows_n)
        gacc[at, :] = jnp.zeros((rows_n, F), f32)
        vacc[at, :] = jnp.zeros((rows_n, F), f32)

    tok_copy().wait_recv()
    norm_rows(peer, T)

    rows_m = 256

    def up_pair(c, buf, acc, t):
        k1, k2 = t - 1, (2 * n - 2 - t) % n
        cross_in(k1, c).wait_recv()
        when(t < n - 1, lambda: cross_in(k2, c).wait_recv())
        j1, j2 = origin(k1), origin(k2)

        @pl.loop(0, 2 * T // rows_m)
        def _(i):
            at = pl.ds(pl.multiple_of(i * rows_m, rows_m), rows_m)
            acc[at, :] += jnp.dot(nbuf[j1, at, :], buf[k1], preferred_element_type=f32) + jnp.dot(
                nbuf[j2, at, :], buf[k2], preferred_element_type=f32
            )

    @pl.loop(0, n - 2)
    def _(s):
        pump(s, 0)
        pl.when(s >= half)(lambda: up_pair(0, gbuf, gacc, s))
        pump(s, 1)
        pl.when(s >= half)(lambda: up_pair(1, vbuf, vacc, s))

    pump(n - 2, 0)
    pump(n - 2, 1)

    def pump_down(u):
        if u < half:
            pump(u, 2)
            pump(u, 3)

    pump_down(0)
    up_pair(0, gbuf, gacc, n - 2)
    pump_down(1)
    up_pair(1, vbuf, vacc, n - 2)
    pump_down(2)
    up_pair(0, gbuf, gacc, n - 1)
    pump_down(3)
    up_pair(1, vbuf, vacc, n - 1)

    @pl.loop(0, 2 * T // rows_n)
    def _(i):
        at = pl.ds(pl.multiple_of(i * rows_n, rows_n), rows_n)
        gate = gacc[at, :]
        hid[at, :] = (gate / (1.0 + jnp.exp(-gate)) * vacc[at, :]).astype(bf16)

    def down(k):
        j = origin(k)

        @pl.loop(0, 2 * T // rows_m)
        def _(i):
            at = pl.ds(pl.multiple_of((i * rows_m + T) % (2 * T), rows_m), rows_m)
            nbuf[j, at, :] = jnp.dot(hid[at, :], dbuf[k], preferred_element_type=f32).astype(bf16)

        part_copy(j).start()

    def down_in(k):
        cross_in(k, 2).wait_recv()
        cross_in(k, 3).wait_recv()

    down(n - 1)

    @pl.loop(min(4, half), n - 1)
    def _(u):
        pump(u, 2)
        pump(u, 3)

        @pl.when(u >= half)
        def _():
            down_in(u - 1)
            down(u - 1)
            down_in(n - 2 - u)
            down(n - 2 - u)

    down_in(n - 2)
    down(n - 2)

    @pl.loop(0, n)
    def _(j):
        part_copy(j).wait_recv()

    rows_o = 32

    @pl.loop(0, T // rows_o)
    def _(i):
        at = pl.ds(pl.multiple_of(i * rows_o, rows_o), rows_o)
        total = jnp.zeros((rows_o, 1), f32)
        blocks = []
        for j in range(n):
            block = (nbuf[j, at, :].astype(f32) + precv[j, at, :].astype(f32)).astype(bf16)
            blocks.append(block)
            wide = block.astype(f32)
            total += jnp.sum(wide * wide, -1, keepdims=True)
        scale = lax.rsqrt(total / D + eps_norm)
        branch = jnp.concatenate(blocks, -1).astype(f32)
        updated = tok_ref[at, :].astype(f32) + 0.5 * (branch * scale * post_ref[...].astype(f32))
        out_ref[at, :] = updated.astype(bf16)

    tok_copy().wait_send()

    @pl.loop(0, n)
    def _(j):
        part_copy(j).wait_send()

    @pl.loop(0, n - 1)
    def _(s):
        for c in range(4):
            cw(s, c).wait_send()
            ccw(s, c).wait_send()
            cross(s, c).wait_send()


def shards(n, tokens, pre_gain, gate_weight, value_weight, down_weight, post_gain):
    T, D = tokens.shape
    R, F = gate_weight.shape
    vmem = pl.BlockSpec(memory_space=pltpu.VMEM)
    hbm = pl.BlockSpec(memory_space=pl.ANY)
    dma = pltpu.SemaphoreType.DMA
    return pl.pallas_call(
        functools.partial(kernel, n),
        out_shape=jax.ShapeDtypeStruct((T, D), bf16),
        in_specs=[vmem, vmem, vmem, hbm, hbm, hbm],
        out_specs=vmem,
        scratch_shapes=[
            pltpu.VMEM((n, R, F), bf16),
            pltpu.VMEM((n, R, F), bf16),
            pltpu.VMEM((n, F, R), bf16),
            pltpu.VMEM((n, 2 * T, R), bf16),
            pltpu.VMEM((T, D), bf16),
            pltpu.VMEM((2 * T, F), f32),
            pltpu.VMEM((2 * T, F), f32),
            pltpu.VMEM((2 * T, F), bf16),
            pltpu.VMEM((n, T, R), bf16),
            dma((3, 4, n - 1)),
            dma((3, 4, n - 1)),
            dma((2,)),
            dma((n,)),
            dma((n,)),
            dma((3,)),
        ],
        compiler_params=pltpu.CompilerParams(
            collective_id=0, has_side_effects=True, vmem_limit_bytes=67043328
        ),
    )(tokens, pre_gain.reshape(1, D), post_gain.reshape(1, D), gate_weight, value_weight, down_weight)


def solution(mesh):
    assert mesh.shape["rep"] == 2 and mesh.shape["tp"] == 2
    placed = (P(("rep", "fs", "tp"), None), P(), P("fs", "tp"), P("fs", "tp"), P("tp", "fs"), P())
    return jax.shard_map(
        functools.partial(shards, mesh.shape["fs"]),
        mesh=mesh, in_specs=placed, out_specs=P(("rep", "fs", "tp"), None), check_vma=False,
    )
```

time: 355 us -> 149 us (0.42)
  waiting for transfers between devices: 296 us -> 0 us
  Pallas kernels: 0 us -> 143 us
  matrix products: 32.2 us -> 0 us
  between operations: 13.2 us -> 0.01 us
  other arithmetic: 12.4 us -> 0 us
  local copies, waits for them, and re-layouts: 0.66 us -> 5.74 us
    all_gather x4 -> x0, waiting for transfers between devices: 282 us -> none  [the longest x1 93.8 us: shards(): lax.all_gather(gate_weight, 'fs', axis=0, tiled=True)]
    pallas_call x0 -> x1, Pallas kernels: none -> 143 us  [shards(): pl.pallas_call(functools.partial(kernel, n), out_shape=jax.ShapeDtypeStru...]
    dot_general x2 -> x0, matrix products: 32.2 us -> none  [the longest x1 20.6 us: shards(): jnp.dot(hidden, down_full, preferred_element_type=jnp.float32)]
    reduce_scatter x1 -> x0, waiting for transfers between devices: 11.7 us -> none  [shards(): lax.psum_scatter(jnp.dot(hidden, down_full, preferred_element_type=jnp.fl...]
    convert_element_type x4 -> x0, other arithmetic: 8.2 us -> none  [the longest x1 4.05 us: shards(): return updated.astype(jnp.bfloat16)]
    reduce_sum x2 -> x0, other arithmetic: 4.15 us -> none  [rms_rows(): jnp.mean(floats * floats, -1, keepdims=True) + eps_norm]
  transfers between devices with their start and end apart: 5 -> 0, of which waited for: 5 -> 0; matrix products, arithmetic and copies ran while one was open for 3% -> 0% of each run, Pallas kernels for 0% -> 0%
where the time goes in v1:
time: 149 us; the launch traced here: 148 us
  Pallas kernels  143 us (96%)
  local copies, waits for them, and re-layouts  5.74 us (4%)
    pallas_call x1, Pallas kernels, shards(): pl.pallas_call(functools.partial(kernel, n), out_shape=jax.ShapeDtypeStru...  143 us
    unnamed x1, local copies, waits for them, and re-layouts  3.16 us

profile of v1, /device:TPU:1, one launch (start us, length us, event | category | flops | bytes accessed | tf_op | source)
XLA Modules:
  0.0 148.4 jit_solution(4718077545497097350)
XLA Ops:
  0.0 1.3 reshape.6.pre_ref
  1.3 1.3 reshape.7.post_ref
  2.6 142.6 %shard_map.64 = bf16[512,2048]{1,0:T(8,128)(2,1)} custom-call(bf16[512,2048]{1,0:T(8,128)(2,1)} %tok_ref.1, bf16[1,2048]{1,0:T(2,128)(2,1)} %reshape.6.pre_ref, bf16[1,2048]{1,0:T(2,128)(2,1)} %reshape.7.post_ref, bf16[256,1408]{1,0:T(8,128)(2,1)} %g_ref.1, bf16[256,1408]{1,0:T(8,128)(2,1)} %v_ref.1, bf16[1408,256]{1,0:T(8,128)(2,1)} %d_ref.1), custom_call_target="tpu_custom_call" | custom-call | tf_op jit(solution)/shard_map/pallas_call | solution.py:273
  145.2 3.2 %copy.8 = bf16[512,2048]{1,0:T(8,128)(2,1)} copy(bf16[512,2048]{1,0:T(8,128)(2,1)} %shard_map.64) | data formatting | bytes 4194304

commit v2 on v1

--- a/solution.py
+++ b/solution.py
@@ -13,12 +13,25 @@
 bf16 = jnp.bfloat16
 
 
-def third(rows):
-    return max(rows // 3 // 16, 1) * 16
-
-
-def half_of(rows):
-    return (rows // 2 + 15) // 16 * 16
+def ring_rows(R, F):
+    gate = max(R // 48, 1) * 16
+    value = min((R + 47) // 48 * 16, (R - 16) // 32 * 16)
+    down = min(round((R - gate - value) * F / R / 16) * 16, (F - 128) // 32 * 16)
+    return gate, value, down
+
+
+UP_CUTS, DOWN_CUTS = 2, 2
+
+
+def cut(rows, pieces):
+    tiles = rows // 16
+    edges = [tiles * i // pieces * 16 for i in range(pieces)] + [rows]
+    return [(low, high - low) for low, high in zip(edges, edges[1:])]
+
+
+def up_cuts(R, F):
+    gate, value, _ = ring_rows(R, F)
+    return min(UP_CUTS, gate // 16, (R - 2 * value) // 16)
 
 
 def when(condition, action):
@@ -30,9 +43,9 @@
 
 
 def kernel(
-    n, tok_ref, pre_ref, post_ref, g_ref, v_ref, d_ref, out_ref,
+    n, tok_ref, pre_ref, g_ref, v_ref, d_ref, branch_ref,
     gbuf, vbuf, dbuf, nbuf, peer, gacc, vacc, hid, precv,
-    send_sem, recv_sem, tok_sem, part_send, part_recv, own_sem,
+    send_sem, recv_sem, tok_sem, part_send, part_recv, own_sem, branch_sem,
 ):
     T, D = tok_ref.shape
     R = gbuf.shape[1]
@@ -56,14 +69,17 @@
     def origin(k):
         return fs_at((pos + 2 * n - 1 - k) % n)
 
-    a, b = third(R), third(F)
-    b0, c0 = half_of(b), half_of(F - 2 * b)
-    chunks = (
-        (gbuf, a, 0, a, 2 * a, R - 2 * a),
-        (vbuf, a, 0, a, 2 * a, R - 2 * a),
-        (dbuf, b, 0, b0, 2 * b, c0),
-        (dbuf, b, b0, b - b0, 2 * b + c0, F - 2 * b - c0),
-    )
+    def cuts(buf, rows, size, pieces):
+        return [
+            (buf, size, low, length, 2 * size + low_c, length_c)
+            for (low, length), (low_c, length_c) in zip(cut(size, pieces), cut(rows - 2 * size, pieces))
+        ]
+
+    ups = up_cuts(R, F)
+    sizes = ring_rows(R, F)
+    chunks = cuts(gbuf, R, sizes[0], ups) + cuts(vbuf, R, sizes[1], ups) + cuts(dbuf, F, sizes[2], DOWN_CUTS)
+    gate_set, value_set = range(ups), range(ups, 2 * ups)
+    down_set = range(2 * ups, 2 * ups + DOWN_CUTS)
 
     def part(c, k, which):
         buf, size, start, length = chunks[c][:4]
@@ -122,11 +138,11 @@
         pl.semaphore_signal(barrier, inc=1, device_id=to, device_id_type=MESH)
     pl.semaphore_wait(barrier, 4)
 
-    for c in range(4):
-        if c < 3:
-            own[c].wait()
-        cw(0, c).start()
-        ccw(0, c).start()
+    for copy, owned in zip(own, (gate_set, value_set, down_set)):
+        copy.wait()
+        for c in owned:
+            cw(0, c).start()
+            ccw(0, c).start()
     tok_copy().start()
 
     rows_n = 64
@@ -136,7 +152,7 @@
         def _(i):
             at = pl.ds(pl.multiple_of(i * rows_n, rows_n), rows_n)
             x = src[at, :].astype(f32)
-            x = x * lax.rsqrt(jnp.mean(x * x, -1, keepdims=True) + eps_norm) * pre_ref[...].astype(f32)
+            x = x * lax.rsqrt(jnp.mean(x * x, -1, keepdims=True) + eps_norm) * pre_ref[...].astype(f32)[None, :]
             x = x.astype(bf16)
             to = pl.ds(pl.multiple_of(base + i * rows_n, rows_n), rows_n)
             for j in range(n):
@@ -155,42 +171,48 @@
 
     rows_m = 256
 
-    def up_pair(c, buf, acc, t):
+    tiles_m = 2 * T // rows_m
+
+    def up_pair(owned, t, piece, pieces):
+        buf, acc = (gbuf, gacc) if owned is gate_set else (vbuf, vacc)
         k1, k2 = t - 1, (2 * n - 2 - t) % n
-        cross_in(k1, c).wait_recv()
-        when(t < n - 1, lambda: cross_in(k2, c).wait_recv())
+        if piece == 0:
+            for c in owned:
+                cross_in(k1, c).wait_recv()
+                when(t < n - 1, lambda: cross_in(k2, c).wait_recv())
         j1, j2 = origin(k1), origin(k2)
 
-        @pl.loop(0, 2 * T // rows_m)
+        @pl.loop(tiles_m * piece // pieces, tiles_m * (piece + 1) // pieces)
         def _(i):
             at = pl.ds(pl.multiple_of(i * rows_m, rows_m), rows_m)
             acc[at, :] += jnp.dot(nbuf[j1, at, :], buf[k1], preferred_element_type=f32) + jnp.dot(
                 nbuf[j2, at, :], buf[k2], preferred_element_type=f32
             )
 
-    @pl.loop(0, n - 2)
+    @pl.loop(0, n - 1)
     def _(s):
-        pump(s, 0)
-        pl.when(s >= half)(lambda: up_pair(0, gbuf, gacc, s))
-        pump(s, 1)
-        pl.when(s >= half)(lambda: up_pair(1, vbuf, vacc, s))
-
-    pump(n - 2, 0)
-    pump(n - 2, 1)
+        for i, c in enumerate(gate_set):
+            pump(s, c)
+            pl.when(s > half)(lambda: up_pair(value_set, s - 1, i, ups))
+        for i, c in enumerate(value_set):
+            pump(s, c)
+            pl.when(s >= half)(lambda: up_pair(gate_set, s, i, ups))
 
     def pump_down(u):
-        if u < half:
-            pump(u, 2)
-            pump(u, 3)
-
+        for c in down_set:
+            pump(u, c)
+
+    early = min(4, half)
     pump_down(0)
-    up_pair(0, gbuf, gacc, n - 2)
-    pump_down(1)
-    up_pair(1, vbuf, vacc, n - 2)
-    pump_down(2)
-    up_pair(0, gbuf, gacc, n - 1)
-    pump_down(3)
-    up_pair(1, vbuf, vacc, n - 1)
+    up_pair(value_set, n - 2, 0, 1)
+    if early > 1:
+        pump_down(1)
+    up_pair(gate_set, n - 1, 0, 1)
+    if early > 2:
+        pump_down(2)
+    up_pair(value_set, n - 1, 0, 1)
+    if early > 3:
+        pump_down(3)
 
     @pl.loop(0, 2 * T // rows_n)
     def _(i):
@@ -209,15 +231,14 @@
         part_copy(j).start()
 
     def down_in(k):
-        cross_in(k, 2).wait_recv()
-        cross_in(k, 3).wait_recv()
+        for c in down_set:
+            cross_in(k, c).wait_recv()
 
     down(n - 1)
 
-    @pl.loop(min(4, half), n - 1)
+    @pl.loop(early, n - 1)
     def _(u):
-        pump(u, 2)
-        pump(u, 3)
+        pump_down(u)
 
         @pl.when(u >= half)
         def _():
@@ -229,26 +250,29 @@
     down_in(n - 2)
     down(n - 2)
 
+    def finish(k):
+        j = origin(k)
+        part_copy(j).wait_recv()
+
+        @pl.loop(0, T // rows_n)
+        def _(i):
+            at = pl.ds(pl.multiple_of(i * rows_n, rows_n), rows_n)
+            nbuf[j, at, :] = (nbuf[j, at, :].astype(f32) + precv[j, at, :].astype(f32)).astype(bf16)
+
+        branch_copy(j).start()
+
+    def branch_copy(j):
+        return pltpu.make_async_copy(nbuf.at[j, pl.ds(0, T)], branch_ref.at[j], branch_sem.at[j])
+
+    finish(n - 1)
+
+    @pl.loop(0, n - 1)
+    def _(k):
+        finish(k)
+
     @pl.loop(0, n)
     def _(j):
-        part_copy(j).wait_recv()
-
-    rows_o = 32
-
-    @pl.loop(0, T // rows_o)
-    def _(i):
-        at = pl.ds(pl.multiple_of(i * rows_o, rows_o), rows_o)
-        total = jnp.zeros((rows_o, 1), f32)
-        blocks = []
-        for j in range(n):
-            block = (nbuf[j, at, :].astype(f32) + precv[j, at, :].astype(f32)).astype(bf16)
-            blocks.append(block)
-            wide = block.astype(f32)
-            total += jnp.sum(wide * wide, -1, keepdims=True)
-        scale = lax.rsqrt(total / D + eps_norm)
-        branch = jnp.concatenate(blocks, -1).astype(f32)
-        updated = tok_ref[at, :].astype(f32) + 0.5 * (branch * scale * post_ref[...].astype(f32))
-        out_ref[at, :] = updated.astype(bf16)
+        branch_copy(j).wait()
 
     tok_copy().wait_send()
 
@@ -258,10 +282,23 @@
 
     @pl.loop(0, n - 1)
     def _(s):
-        for c in range(4):
+        for c in range(len(chunks)):
             cw(s, c).wait_send()
             ccw(s, c).wait_send()
             cross(s, c).wait_send()
+
+
+def add_normed(branch_ref, tok_ref, post_ref, out_ref):
+    n, rows, R = branch_ref.shape
+    D = tok_ref.shape[1]
+    total = jnp.zeros((rows, 1), f32)
+    for j in range(n):
+        wide = branch_ref[j].astype(f32)
+        total += jnp.sum(wide * wide, -1, keepdims=True)
+    scale = 0.5 * lax.rsqrt(total / D + eps_norm)
+    branch = jnp.concatenate([branch_ref[j] for j in range(n)], -1).astype(f32)
+    updated = tok_ref[...].astype(f32) + branch * scale * post_ref[...].astype(f32)[None, :]
+    out_ref[...] = updated.astype(bf16)
 
 
 def shards(n, tokens, pre_gain, gate_weight, value_weight, down_weight, post_gain):
@@ -270,11 +307,11 @@
     vmem = pl.BlockSpec(memory_space=pltpu.VMEM)
     hbm = pl.BlockSpec(memory_space=pl.ANY)
     dma = pltpu.SemaphoreType.DMA
-    return pl.pallas_call(
+    branch = pl.pallas_call(
         functools.partial(kernel, n),
-        out_shape=jax.ShapeDtypeStruct((T, D), bf16),
-        in_specs=[vmem, vmem, vmem, hbm, hbm, hbm],
-        out_specs=vmem,
+        out_shape=jax.ShapeDtypeStruct((n, T, R), bf16),
+        in_specs=[vmem, vmem, hbm, hbm, hbm],
+        out_specs=hbm,
         scratch_shapes=[
             pltpu.VMEM((n, R, F), bf16),
             pltpu.VMEM((n, R, F), bf16),
@@ -285,17 +322,30 @@
             pltpu.VMEM((2 * T, F), f32),
             pltpu.VMEM((2 * T, F), bf16),
             pltpu.VMEM((n, T, R), bf16),
-            dma((3, 4, n - 1)),
-            dma((3, 4, n - 1)),
+            dma((3, 2 * up_cuts(R, F) + DOWN_CUTS, n - 1)),
+            dma((3, 2 * up_cuts(R, F) + DOWN_CUTS, n - 1)),
             dma((2,)),
             dma((n,)),
             dma((n,)),
             dma((3,)),
+            dma((n,)),
         ],
         compiler_params=pltpu.CompilerParams(
             collective_id=0, has_side_effects=True, vmem_limit_bytes=67043328
         ),
-    )(tokens, pre_gain.reshape(1, D), post_gain.reshape(1, D), gate_weight, value_weight, down_weight)
+    )(tokens, pre_gain, gate_weight, value_weight, down_weight)
+    rows = 128
+    return pl.pallas_call(
+        add_normed,
+        grid=(T // rows,),
+        out_shape=jax.ShapeDtypeStruct((T, D), bf16),
+        in_specs=[
+            pl.BlockSpec((n, rows, R), lambda i: (0, i, 0)),
+            pl.BlockSpec((rows, D), lambda i: (i, 0)),
+            pl.BlockSpec((D,), lambda i: (0,)),
+        ],
+        out_specs=pl.BlockSpec((rows, D), lambda i: (i, 0)),
+    )(branch, tokens, post_gain)
 
 
 def solution(mesh):

time: 149 us -> 138 us (0.926)
  Pallas kernels: 143 us -> 137 us
  local copies, waits for them, and re-layouts: 5.74 us -> 0 us
    pallas_call x1, Pallas kernels: 143 us -> 132 us  [shards(): pl.pallas_call(functools.partial(kernel, n), out_shape=jax.ShapeDtypeStru...]
    pallas_call x0 -> x1, Pallas kernels: none -> 4.94 us  [shards(): pl.pallas_call(add_normed, grid=(T // rows,), out_shape=jax.ShapeDtypeStr...]
    unnamed x1 -> x0, local copies, waits for them, and re-layouts: 3.16 us -> none
    reshape x2 -> x0, local copies, waits for them, and re-layouts: 2.58 us -> none  [the longest x1 1.29 us: shards(): pre_gain.reshape(1, D)]
where the time goes in v2:
time: 138 us; the launch traced here: 137 us
  Pallas kernels  137 us (99%)
    pallas_call x1, Pallas kernels, shards(): pl.pallas_call(functools.partial(kernel, n), out_shape=jax.ShapeDtypeStru...  132 us
    pallas_call x1, Pallas kernels, shards(): pl.pallas_call(add_normed, grid=(T // rows,), out_shape=jax.ShapeDtypeStr...  4.94 us

profile of v2, /device:TPU:1, one launch (start us, length us, event | category | flops | bytes accessed | tf_op | source)
XLA Modules:
  0.0 137.4 jit_solution(12053004945977229717)
XLA Ops:
  0.0 132.5 %shard_map.64.branch_ref = bf16[8,512,256]{2,1,0:T(8,128)(2,1)} custom-call(bf16[512,2048]{1,0:T(8,128)(2,1)} %tok_ref.3, bf16[2048]{0:T(1024)(128)(2,1)} %pre_ref.1, bf16[256,1408]{1,0:T(8,128)(2,1)} %g_ref.1, bf16[256,1408]{1,0:T(8,128)(2,1)} %v_ref.1, bf16[1408,256]{1,0:T(8,128)(2,1)} %d_ref.1), custom_call_target="tpu_custom_call" | custom-call | tf_op jit(solution)/shard_map/pallas_call | solution.py:310
  132.5 4.9 %shard_map.65 = bf16[512,2048]{1,0:T(8,128)(2,1)} custom-call(bf16[8,512,256]{2,1,0:T(8,128)(2,1)} %shard_map.64.branch_ref, bf16[512,2048]{1,0:T(8,128)(2,1)} %tok_ref.3, bf16[2048]{0:T(1024)(128)(2,1)} %post_ref.1), custom_call_target="tpu_custom_call" | custom-call | tf_op jit(solution)/shard_map/pallas_call | solution.py:338
